TPU v7x, 32 devices: a whole 2x2x4 slice. The times are simulated.
32 devices in a mesh: sp: 8 (over z, x), dp: 4 (over y, core).
Axes of the slice: x: 2, y: 2, z: 4, core: 2. Of those that a mesh axis runs over, the one named last changes fastest.
Arguments:
- tokens: bfloat16 [4, 3072, 2048], P('dp', 'sp'), may hold values from -6 to 6
- q_weight: bfloat16 [2048, 1024], P(('sp', 'dp')), may hold values from -0.13258252 to 0.13258252
- k_weight: bfloat16 [2048, 256], P(('sp', 'dp')), may hold values from -0.13258252 to 0.13258252
- v_weight: bfloat16 [2048, 256], P(('sp', 'dp')), may hold values from -0.125 to 0.125
- out_weight: bfloat16 [1024, 2048], P(None, ('sp', 'dp')), may hold values from -6 to 6
- q_gain: float32 [64], replicated, may hold values from 0.5 to 8
- k_gain: float32 [64], replicated, may hold values from 0.5 to 8
Outputs:
- mixed: bfloat16 [4, 3072, 2048], P('dp', 'sp')
All inputs are finite; a program needn't handle non-finite values.
Results may differ from a plain program's by a relative error of at most 0.0055.
The roundings to bfloat16 on the way count: a program that leaves them out, or rounds other values in their place, can miss the bound.
Values may be sent and summed in bfloat16 or wider, within the bound.
A program may use at most 128 MiB of HBM per device.

v0:
```python
import functools
import math

import jax
import jax.numpy as jnp
from jax import lax
from jax.experimental import pallas as pl
from jax.experimental.pallas import tpu as pltpu
from jax.sharding import PartitionSpec as P

GRID_W = 64
CORES = 2
epsilon = 1e-06
rope_base = 10000.0
VMEM_BYTES = 60 * 1024 * 1024


def tables(tok_count, head_width, offset, width):
    quarter = head_width // 4
    positions = jnp.arange(tok_count, dtype=jnp.int32) + offset
    frequency = rope_base ** (-jnp.arange(quarter, dtype=jnp.float32) / quarter)
    row_angle = (positions // GRID_W).astype(jnp.float32)[:, None] * frequency[None, :]
    col_angle = (positions % GRID_W).astype(jnp.float32)[:, None] * frequency[None, :]
    cos = jnp.concatenate([jnp.cos(row_angle)] * 2 + [jnp.cos(col_angle)] * 2, axis=1)
    sin_r, sin_c = jnp.sin(row_angle), jnp.sin(col_angle)
    sin = jnp.concatenate([-sin_r, sin_r, -sin_c, sin_c], axis=1)
    return jnp.tile(cos, (1, width // head_width)), jnp.tile(sin, (1, width // head_width))


class Net:
    def __init__(self, dims):
        self.zs, self.xs, self.ys = dims
        sp, dp = lax.axis_index("sp"), lax.axis_index("dp")
        self.z, self.x = sp // self.xs, sp % self.xs
        self.y, self.c = dp // CORES, dp % CORES
        self.ox, self.oy, self.oc = 1 - self.x, 1 - self.y, 1 - self.c

    def at(self, z=None, x=None, y=None, c=None):
        z = self.z if z is None else z
        x = self.x if x is None else x
        y = self.y if y is None else y
        c = self.c if c is None else c
        return {"sp": z * self.xs + x, "dp": y * CORES + c}

    def sides(self):
        return ((-1, 1), (1, -1))

    def inside(self, z):
        return jnp.logical_and(z >= 0, z < self.zs)


def greet(net, fixed):
    barrier = pltpu.get_barrier_semaphore()
    for where in fixed:
        pl.semaphore_signal(barrier, inc=1, device_id=where, device_id_type=pl.DeviceIdType.MESH)
    for step in (-1, 1):

        @pl.when(net.inside(net.z + step))
        def _():
            pl.semaphore_signal(
                barrier,
                inc=1,
                device_id=net.at(z=net.z + step),
                device_id_type=pl.DeviceIdType.MESH,
            )

    along = jnp.minimum(net.z, 1) + jnp.minimum(net.zs - 1 - net.z, 1)
    pl.semaphore_wait(barrier, len(fixed) + along)


def remote(src, dst, send, recv, where):
    return pltpu.make_async_remote_copy(
        src_ref=src,
        dst_ref=dst,
        send_sem=send,
        recv_sem=recv,
        device_id=where,
        device_id_type=pl.DeviceIdType.MESH,
    )


def gather_weights(net, w_own, wbuf, own_sem, zs_sem, zr_sem, xs, xr, ys, yr, ds, dr, cs, cr):
    half = wbuf.shape[-1] // 2
    halves = (pl.ds(0, half), pl.ds(half, half))

    def block(z, x, y, c):
        return wbuf.at[z, x, y, c]

    def part(z, x, y, c, h):
        return wbuf.at[z, x, y, c, :, halves[h]]

    def to_x(k, z, src=None):
        dst = block(z, net.x, net.y, net.c)
        return remote(dst if src is None else src, dst, xs.at[k], xr.at[k], net.at(x=net.ox))

    def from_x(k, z):
        b = block(z, net.ox, net.y, net.c)
        return remote(b, b, xs.at[k], xr.at[k], net.at(x=net.ox))

    def to_y(k, z, src=None):
        dst = block(z, net.x, net.y, net.c)
        return remote(dst if src is None else src, dst, ys.at[k], yr.at[k], net.at(y=net.oy))

    def from_y(k, z):
        b = block(z, net.x, net.oy, net.c)
        return remote(b, b, ys.at[k], yr.at[k], net.at(y=net.oy))

    def diag_to(k, z, h):
        if h == 0:
            b = part(z, net.ox, net.y, net.c, 0)
            return remote(b, b, ds.at[0, k], dr.at[0, k], net.at(y=net.oy))
        b = part(z, net.x, net.oy, net.c, 1)
        return remote(b, b, ds.at[1, k], dr.at[1, k], net.at(x=net.ox))

    def diag_from(k, z, h):
        b = part(z, net.ox, net.oy, net.c, h)
        where = net.at(y=net.oy) if h == 0 else net.at(x=net.ox)
        return remote(b, b, ds.at[h, k], dr.at[h, k], where)

    def core(kind, k, z, c, src=None):
        x = net.ox if kind in (1, 3, 4) else net.x
        y = net.oy if kind in (2, 3, 4) else net.y
        b = part(z, x, y, c, kind - 3) if kind >= 3 else block(z, x, y, c)
        return remote(
            b if src is None else src, b, cs.at[kind, k], cr.at[kind, k], net.at(c=net.oc)
        )

    def to_z(k, z, step, src=None):
        dst = block(z, net.x, net.y, net.c)
        return remote(
            dst if src is None else src, dst, zs_sem.at[k], zr_sem.at[k], net.at(z=net.z + step)
        )

    def slots():
        for step in range(net.zs - 1):
            for side in range(2):
                sign = -1 if side == 0 else 1
                yield step, side, 1 + 2 * step + side, net.z + sign * (step + 1), -sign

    def spread(k, z, src=None):
        to_x(k, z, src).start()
        to_y(k, z, src).start()
        core(0, k, z, net.c, src).start()

    def second(k, z):
        from_x(k, z).wait_recv()
        diag_to(k, z, 0).start()
        core(1, k, z, net.c).start()
        from_y(k, z).wait_recv()
        diag_to(k, z, 1).start()
        core(2, k, z, net.c).start()

    def third(k, z):
        diag_from(k, z, 0).wait_recv()
        core(3, k, z, net.c).start()
        diag_from(k, z, 1).wait_recv()
        core(4, k, z, net.c).start()

    mine = pltpu.make_async_copy(w_own, block(net.z, net.x, net.y, net.c), own_sem)
    mine.start()
    for side, step in ((0, 1), (1, -1)):

        @pl.when(net.inside(net.z + step))
        def _():
            to_z(1 + side, net.z, step, w_own).start()

    spread(0, net.z, w_own)
    stages = [[(0, net.z)]]
    for s in range(net.zs - 1):
        here = []
        for step, side, k, z, onward in slots():
            if step != s:
                continue

            @pl.when(net.inside(z))
            def _():
                to_z(k, z, 0).wait_recv()
                if s < net.zs - 2:

                    @pl.when(net.inside(net.z + onward))
                    def _():
                        to_z(k + 2, z, onward).start()

                spread(k, z)

            here.append((k, z))
        for k, z in stages[-1]:

            @pl.when(net.inside(z))
            def _():
                second(k, z)

        if len(stages) > 1:
            for k, z in stages[-2]:

                @pl.when(net.inside(z))
                def _():
                    third(k, z)

        stages.append(here)
    for k, z in stages[-1]:

        @pl.when(net.inside(z))
        def _():
            second(k, z)

    for stage in stages[-2:]:
        for k, z in stage:

            @pl.when(net.inside(z))
            def _():
                third(k, z)

    for stage in stages:
        for k, z in stage:

            @pl.when(net.inside(z))
            def _():
                for kind in range(5):
                    core(kind, k, z, net.oc).wait_recv()

    def drain():
        mine.wait()
        for side, step in ((0, 1), (1, -1)):

            @pl.when(net.inside(net.z + step))
            def _():
                to_z(1 + side, net.z, step, w_own).wait_send()

        for step, side, k, z, onward in slots():
            if step < net.zs - 2:

                @pl.when(jnp.logical_and(net.inside(z), net.inside(net.z + onward)))
                def _():
                    to_z(k + 2, z, onward).wait_send()

        for stage in stages:
            for k, z in stage:

                @pl.when(net.inside(z))
                def _():
                    to_x(k, z).wait_send()
                    to_y(k, z).wait_send()
                    diag_to(k, z, 0).wait_send()
                    diag_to(k, z, 1).wait_send()
                    for kind in range(5):
                        core(kind, k, z, net.c).wait_send()

    drain()


def exchange(net, own, buf, own_sem, zs_sem, zr_sem, xs, xr):
    last = 2 * (net.zs - 1)

    def block(z, x):
        return buf.at[z, x]

    def to_z(k, z, step, src=None):
        dst = block(z, net.x)
        return remote(
            dst if src is None else src, dst, zs_sem.at[k], zr_sem.at[k], net.at(z=net.z + step)
        )

    def to_x(k, z, src=None):
        dst = block(z, net.x)
        return remote(dst if src is None else src, dst, xs.at[k], xr.at[k], net.at(x=net.ox))

    def from_x(k, z):
        b = block(z, net.ox)
        return remote(b, b, xs.at[k], xr.at[k], net.at(x=net.ox))

    def owner(k):
        return net.z + jnp.where(k % 2 == 1, -1, 1) * ((k + 1) // 2)

    def goes_on(k):
        return jnp.logical_and(k + 2 <= last, net.inside(net.z + jnp.where(k % 2 == 1, 1, -1)))

    mine = pltpu.make_async_copy(own, block(net.z, net.x), own_sem)

    def start():
        mine.start()
        for side, step in ((0, 1), (1, -1)):

            @pl.when(net.inside(net.z + step))
            def _():
                to_z(1 + side, net.z, step, own).start()

        to_x(0, net.z, own).start()

    def pass_on(k):
        z = owner(k)

        @pl.when(jnp.logical_and(k <= last, net.inside(z)))
        def _():
            to_z(k, z, 0).wait_recv()

            @pl.when(goes_on(k))
            def _():
                to_z(k + 2, z, jnp.where(k % 2 == 1, 1, -1)).start()

            to_x(k, z).start()

    def drain():
        for side, step in ((0, 1), (1, -1)):

            @pl.when(net.inside(net.z + step))
            def _():
                to_z(1 + side, net.z, step, own).wait_send()

        to_x(0, net.z, own).wait_send()

        def one(k, carry):
            z = owner(k)

            @pl.when(net.inside(z))
            def _():
                to_x(k, z).wait_send()

                @pl.when(goes_on(k))
                def _():
                    to_z(k + 2, z, jnp.where(k % 2 == 1, 1, -1)).wait_send()

            return carry

        lax.fori_loop(1, last + 1, one, 0)

    return mine, owner, from_x, start, pass_on, drain


def layer_kernel(
    dims, group, scale, head_width, tok_ref, w_own, cos_ref, sin_ref, gain_ref, out_ref,
    wbuf, q_ref, kv_ref, buf, acc_ref, max_ref, sum_ref, *sems
):
    net = Net(dims)
    greet(net, (net.at(x=net.ox), net.at(y=net.oy), net.at(c=net.oc)))
    gather_weights(net, w_own, wbuf, *sems[:11])
    mine, owner, from_x, start, pass_on, drain = exchange(net, kv_ref, buf, *sems[11:])
    rows, width = cos_ref.shape
    depth = tok_ref.shape[1]
    kv_width = kv_ref.shape[1] // 2
    pair = 2 * head_width
    r = lax.broadcasted_iota(jnp.int32, (width, width), 0) // head_width
    c = lax.broadcasted_iota(jnp.int32, (width, width), 1) // head_width
    averager = jnp.where(r == c, 1.0 / head_width, 0.0).astype(jnp.float32)
    lane = lax.broadcasted_iota(jnp.int32, (rows, width), 1)
    first = lane % (head_width // 2) < head_width // 4
    low = lax.broadcasted_iota(jnp.int32, (rows, pair), 1) < head_width

    def product(at):
        w = wbuf[:, :, :, :, :, at : at + width].reshape(depth, width)
        return jnp.dot(tok_ref[...], w, preferred_element_type=jnp.float32)

    def turned(t, gain):
        mean_sq = jnp.dot(
            t * t, averager, precision=lax.Precision.HIGHEST, preferred_element_type=jnp.float32
        )
        t = t * lax.rsqrt(mean_sq + epsilon) * gain
        quarter = head_width // 4
        other = jnp.where(first, pltpu.roll(t, width - quarter, 1), pltpu.roll(t, quarter, 1))
        return t * cos_ref[...] + other * sin_ref[...]

    per = width // head_width
    for j in range(kv_width // width):
        k = turned(product(j * width), gain_ref[1:2, :])
        v = product(kv_width + j * width)
        for i in range(0, per, 2):
            kp = k[:, i * head_width : i * head_width + pair]
            vp = v[:, i * head_width : i * head_width + pair]
            at = (j * per + i) * pair
            kv_ref[:, at : at + pair] = jnp.where(low, kp, pltpu.roll(vp, head_width, 1)).astype(
                kv_ref.dtype
            )
            kv_ref[:, at + pair : at + 2 * pair] = jnp.where(
                low, pltpu.roll(kp, head_width, 1), vp
            ).astype(kv_ref.dtype)
    max_ref[...] = jnp.full_like(max_ref, -jnp.inf)
    sum_ref[...] = jnp.zeros_like(sum_ref)
    acc_ref[...] = jnp.zeros_like(acc_ref)
    for j in range(q_ref.shape[0] // per):
        if j == 1:
            start()
        q = turned(product(2 * kv_width + j * width), gain_ref[0:1, :])
        q = q.astype(q_ref.dtype).astype(jnp.float32) * scale
        for i in range(0, per, 2):
            qp = q[:, i * head_width : i * head_width + pair]
            q_ref[j * per + i] = jnp.where(low, qp, 0.0).astype(q_ref.dtype)
            q_ref[j * per + i + 1] = jnp.where(low, pltpu.roll(qp, head_width, 1), 0.0).astype(
                q_ref.dtype
            )

    block = 128 if rows % 128 == 0 else rows
    blocks = [pl.ds(i * block, block) for i in range(rows // block)]
    keys_now = buf.shape[1] * rows
    pairs = q_ref.shape[0] // 2

    def update(h, keys, old, total, acc):
        s = lax.dot_general(
            q_ref[h], keys, (((1,), (1,)), ((), ())), preferred_element_type=jnp.float32
        )
        top = jnp.maximum(old, jnp.max(s, axis=-1, keepdims=True))
        p = jnp.exp(s - jnp.concatenate([top] * (keys_now // pair), axis=1))
        fade = jnp.exp(old - top)
        total = total * fade + jnp.sum(p, axis=-1, keepdims=True)
        acc = acc * fade + jnp.dot(
            p.astype(keys.dtype), keys, preferred_element_type=jnp.float32
        )
        return top, total, acc

    def attend(z):
        def step(j, carry):
            g = j // (group // 2)
            keys = buf[z, :, :, pl.ds(pl.multiple_of(g * pair, pair), pair)]
            keys = keys.reshape(keys_now, pair)
            two = (2 * j, 2 * j + 1)
            state = [(max_ref[h], sum_ref[h], acc_ref[h]) for h in two]
            state = [update(h, keys, *held) for h, held in zip(two, state)]
            for h, (top, total, acc) in zip(two, state):
                max_ref[h] = top
                sum_ref[h] = total
                acc_ref[h] = acc
            return carry

        lax.fori_loop(0, pairs, step, 0)

    pass_on(1)
    pass_on(2)
    mine.wait()

    def arrival(k, carry):
        @pl.when(k % 2 == 1)
        def _():
            pass_on(k + 2)
            pass_on(k + 3)

        z = owner(k)

        @pl.when(net.inside(z))
        def _():
            from_x(k, z).wait_recv()
            attend(z)

        return carry

    lax.fori_loop(0, 2 * (net.zs - 1) + 1, arrival, 0)
    low_block = lax.broadcasted_iota(jnp.int32, (block, pair), 1) < head_width

    def finish(j, carry):
        for at in blocks:
            a = acc_ref[2 * j, at, :] / sum_ref[2 * j, at, :]
            b = acc_ref[2 * j + 1, at, :] / sum_ref[2 * j + 1, at, :]
            out_ref[at, pl.ds(pl.multiple_of(j * pair, pair), pair)] = jnp.where(
                low_block, pltpu.roll(a, head_width, 1), b
            ).astype(out_ref.dtype)
        return carry

    lax.fori_loop(0, pairs, finish, 0)
    drain()


def vmem():
    return pl.BlockSpec(memory_space=pltpu.VMEM)


def fast(dims, tokens, q_weight, k_weight, v_weight, out_weight, q_gain, k_gain):
    zs, xs, ys = dims
    rows_in = tokens[0]
    tok_count, depth = rows_in.shape
    head_width = q_gain.shape[0]
    q_heads = out_weight.shape[0] // head_width
    kv_width = k_weight.shape[1]
    group = q_heads // (kv_width // head_width)
    offset = lax.axis_index("sp") * tok_count
    width = 4 * head_width
    cos, sin = tables(tok_count, head_width, offset, width)
    own = jnp.concatenate([k_weight, v_weight, q_weight], axis=1)
    pair = 2 * head_width
    dma = pltpu.SemaphoreType.DMA
    n = 1 + 2 * (zs - 1)
    out_full = lax.all_gather(out_weight, ("sp", "dp"), axis=1, tiled=True)
    attended = pl.pallas_call(
        functools.partial(layer_kernel, dims, group, head_width ** (-0.5), head_width),
        out_shape=jax.ShapeDtypeStruct((tok_count, q_heads * head_width), jnp.bfloat16),
        in_specs=[vmem()] * 5,
        out_specs=vmem(),
        scratch_shapes=[
            pltpu.VMEM((zs, xs, ys, CORES) + own.shape, jnp.bfloat16),
            pltpu.VMEM((q_heads, tok_count, pair), jnp.bfloat16),
            pltpu.VMEM((tok_count, 2 * kv_width), jnp.bfloat16),
            pltpu.VMEM((zs, xs, tok_count, 2 * kv_width), jnp.bfloat16),
            pltpu.VMEM((q_heads, tok_count, pair), jnp.float32),
            pltpu.VMEM((q_heads, tok_count, pair), jnp.float32),
            pltpu.VMEM((q_heads, tok_count, pair), jnp.float32),
            dma,
            dma((n,)), dma((n,)), dma((n,)), dma((n,)), dma((n,)), dma((n,)),
            dma((2, n)), dma((2, n)), dma((5, n)), dma((5, n)),
            dma,
            dma((n,)), dma((n,)), dma((n,)), dma((n,)),
        ],
        compiler_params=pltpu.CompilerParams(
            collective_id=0, has_side_effects=True, vmem_limit_bytes=VMEM_BYTES
        ),
        cost_estimate=pl.CostEstimate(
            flops=100_000_000_000, bytes_accessed=10_000_000, transcendentals=20_000_000
        ),
    )(
        rows_in, own, cos, sin,
        jnp.tile(jnp.stack([q_gain, k_gain]), (1, width // head_width)),
    )
    result = jnp.dot(attended, out_full, preferred_element_type=jnp.float32)
    return result.astype(jnp.bfloat16)[None]


def normalize(tensor, gain_vec):
    mean_sq = jnp.mean(tensor * tensor, axis=-1, keepdims=True)
    return tensor * lax.rsqrt(mean_sq + epsilon) * gain_vec


def rotate(tensor, offset):
    row_count = tensor.shape[0]
    head_width = tensor.shape[2]
    quarter = head_width // 4
    half_width = head_width // 2
    positions = jnp.arange(row_count, dtype=jnp.int32) + offset
    frequency = rope_base ** (-jnp.arange(quarter, dtype=jnp.float32) / quarter)

    def rotate_pair(segment, coords):
        angles = coords.astype(jnp.float32)[:, None] * frequency[None, :]
        cosine = jnp.cos(angles)[:, None, :]
        sine_val = jnp.sin(angles)[:, None, :]
        low_half = segment[..., :quarter]
        high_half = segment[..., quarter:]
        return jnp.concatenate(
            [low_half * cosine - high_half * sine_val, high_half * cosine + low_half * sine_val],
            axis=-1,
        )

    return jnp.concatenate(
        [
            rotate_pair(tensor[..., :half_width], positions // GRID_W),
            rotate_pair(tensor[..., half_width:], positions % GRID_W),
        ],
        axis=-1,
    )


def attend(query_rows, key_rows, value_rows):
    row_count, head_width = query_rows.shape
    block_rows = math.gcd(row_count, 512)
    score_scale = head_width ** (-0.5)

    def attend_block(segment):
        scores = (
            lax.dot_general(
                segment, key_rows, (((1,), (1,)), ((), ())), preferred_element_type=jnp.float32
            )
            * score_scale
        )
        row_max = jnp.max(scores, axis=-1, keepdims=True)
        weights = jnp.exp(scores - row_max)
        shares = (weights / jnp.sum(weights, axis=-1, keepdims=True)).astype(jnp.bfloat16)
        return jnp.dot(shares, value_rows, preferred_element_type=jnp.float32).astype(jnp.bfloat16)

    blocks = query_rows.reshape(row_count // block_rows, block_rows, head_width)
    return lax.map(attend_block, blocks).reshape(row_count, head_width)


def plain(tokens, q_weight, k_weight, v_weight, out_weight, q_gain, k_gain):
    rows_in = tokens[0]
    tok_count = rows_in.shape[0]
    head_width = q_gain.shape[0]
    q_width = out_weight.shape[0]
    kv_width = k_weight.shape[1]
    q_heads = q_width // head_width
    kv_heads = kv_width // head_width
    group_size = q_heads // kv_heads
    sp_count = lax.axis_size("sp")
    offset = lax.axis_index("sp") * tok_count
    weight_rows = (
        lax.all_gather(q_weight, ("sp", "dp"), axis=0, tiled=True),
        lax.all_gather(k_weight, ("sp", "dp"), axis=0, tiled=True),
        lax.all_gather(v_weight, ("sp", "dp"), axis=0, tiled=True),
    )
    query_raw, key_raw, value_raw = tuple(
        (
            jnp.dot(rows_in, rows_part, preferred_element_type=jnp.float32)
            for rows_part in weight_rows
        )
    )
    queries = rotate(
        normalize(query_raw.reshape(tok_count, q_heads, head_width), q_gain), offset
    ).astype(jnp.bfloat16)
    keys_rot = rotate(
        normalize(key_raw.reshape(tok_count, kv_heads, head_width), k_gain), offset
    ).astype(jnp.bfloat16)
    values_dev = value_raw.astype(jnp.bfloat16)
    keys_wide = jnp.broadcast_to(
        keys_rot[:, :, None, :], (tok_count, kv_heads, group_size, head_width)
    ).reshape(tok_count, q_width)
    values_wide = jnp.broadcast_to(
        values_dev.reshape(tok_count, kv_heads, 1, head_width),
        (tok_count, kv_heads, group_size, head_width),
    ).reshape(tok_count, q_width)
    q_local, k_local, v_local = (
        lax.all_to_all(
            queries.reshape(tok_count, q_width), "sp", split_axis=1, concat_axis=0, tiled=True
        ),
        lax.all_to_all(keys_wide, "sp", split_axis=1, concat_axis=0, tiled=True),
        lax.all_to_all(values_wide, "sp", split_axis=1, concat_axis=0, tiled=True),
    )
    local_heads = q_width // sp_count // head_width
    outputs = []
    for head_index in range(local_heads):
        low_col = head_index * head_width
        outputs.append(
            attend(
                q_local[:, low_col : low_col + head_width],
                k_local[:, low_col : low_col + head_width],
                v_local[:, low_col : low_col + head_width],
            )
        )
    head_results = jnp.concatenate(outputs, axis=1)
    attended = lax.all_to_all(head_results, "sp", split_axis=0, concat_axis=1, tiled=True)
    result = jnp.dot(
        attended,
        lax.all_gather(out_weight, ("sp", "dp"), axis=1, tiled=True),
        preferred_element_type=jnp.float32,
    ).astype(jnp.bfloat16)
    return result[None]


def solution(mesh):
    sp, dp = mesh.shape["sp"], mesh.shape["dp"]
    across = dp // CORES
    exchange = dp == 2 * CORES and sp % across == 0 and sp // across > 1
    body = functools.partial(fast, (sp // across, across, across)) if exchange else plain
    return jax.shard_map(
        body,
        mesh=mesh,
        in_specs=(
            P("dp", "sp", None),
            P(("sp", "dp"), None),
            P(("sp", "dp"), None),
            P(("sp", "dp"), None),
            P(None, ("sp", "dp")),
            P(),
            P(),
        ),
        out_specs=P("dp", "sp", None),
        check_vma=False,
    )
```

profile of v0, /device:TPU:0, one launch (start us, length us, event | category | flops | bytes accessed | tf_op | source)
XLA Modules:
  0.0 134.4 jit_solution(1457024559381651107)
XLA Ops:
  6.5 0.0 all-gather.2.cloned.1.call-start
  6.5 0.7 all-gather.2.cloned.1.call-update
  7.3 0.7 pad_maximum_fusion.3
  8.0 0.7 tile.32.gain_ref
  8.7 0.3 fusion.1
  9.0 0.9 copy.8.cos_ref
  9.9 0.9 copy.9.sin_ref
  10.8 1.6 %pad_maximum_fusion.w_own = bf16[64,1536]{1,0:T(8,128)(2,1)} fusion(bf16[64,1024]{1,0:T(8,128)(2,1)} %param.8, bf16[64,256]{1,0:T(8,128)(2,1)} %param.10, bf16[64,256]{1,0:T(8,128)(2,1)} %param.9), kind=kLoop, calls=%fused_computation.2 | loop fusion | flops 589824 | bytes 393216 | tf_op jit(solution)/shard_map/concatenate | solution.py:475
  12.5 109.7 %shard_map.73 = bf16[384,1024]{1,0:T(8,128)(2,1)} custom-call(bf16[384,2048]{1,0:T(8,128)(2,1)} %bitcast.13, bf16[64,1536]{1,0:T(8,128)(2,1)} %pad_maximum_fusion.w_own, f32[384,256]{1,0:T(8,128)} %copy.8.cos_ref, f32[384,256]{1,0:T(8,128)} %copy.9.sin_ref, f32[2,256]{1,0:T(2,128)} %tile.32.gain_ref), custom_call_target="tpu_custom_call" | custom-call | flops 99999997952 | bytes 10000000 | tf_op jit(solution)/shard_map/pallas_call | solution.py:480
  122.2 0.0 all-gather.2.cloned.1.call-done
  122.2 5.4 %fusion = bf16[1,384,2048]{2,1,0:T(8,128)(2,1)} fusion(bf16[384,1024]{1,0:T(8,128)(2,1)} %shard_map.73, bf16[1024,2048]{0,1:T(8,128)(2,1)} %all-gather.2.cloned.1.call-done), kind=kOutput, calls=%fused_computation.1 | convolution fusion | flops 1611399168 | bytes 6553600 | tf_op jit(solution)/shard_map/dot_general | solution.py:509
  (7 shorter events, 0.1 us)
Async XLA Ops:
  6.5 115.7 %all-gather.2.cloned.1.call-start = ((), (), s32[]{:S(2)}) async-start(), calls=%async_computation | async-start | bytes 4325376 | tf_op jit(solution)/shard_map/all_gather | solution.py:479
Sparse Core Ops, SparseCore 0:
  10.2 74.3 all-gather.1
where the time goes:
time: 135 us; the launch traced here: 134 us
  Pallas kernels  110 us (81%)
  between operations  13.4 us (10%)
  matrix products  5.4 us (4%)
  other arithmetic  2.6 us (2%)
  local copies, waits for them, and re-layouts  2.56 us (2%)
    pallas_call x1, Pallas kernels, fast(): pl.pallas_call(functools.partial(layer_kernel, dims, group, head_width **...  110 us
    dot_general x1, matrix products, fast(): result = jnp.dot(attended, out_full, preferred_element_type=jnp.float32)  5.4 us
  transfers between devices with their start and end apart: 1, of which 0 were waited for; matrix products, arithmetic and copies ran while one was open for 4% of the time, Pallas kernels for 82%

commit v1 on v0

v1 whole, which is shorter than its diff:
```python
import functools
import math

import jax
import jax.numpy as jnp
from jax import lax
from jax.experimental import pallas as pl
from jax.experimental.pallas import tpu as pltpu
from jax.sharding import PartitionSpec as P

GRID_W = 64
CORES = 2
epsilon = 1e-06
rope_base = 10000.0
VMEM_BYTES = 60 * 1024 * 1024


class Net:
    def __init__(self, dims):
        self.zs, self.xs, self.ys = dims
        sp, dp = lax.axis_index("sp"), lax.axis_index("dp")
        self.z, self.x = sp // self.xs, sp % self.xs
        self.y, self.c = dp // CORES, dp % CORES
        self.ox, self.oy, self.oc = 1 - self.x, 1 - self.y, 1 - self.c

    def at(self, z=None, x=None, y=None, c=None):
        z = self.z if z is None else z
        x = self.x if x is None else x
        y = self.y if y is None else y
        c = self.c if c is None else c
        return {"sp": z * self.xs + x, "dp": y * CORES + c}

    def near(self, k):
        below, above = self.z, self.zs - 1 - self.z
        both = jnp.minimum(below, above)
        inner = k <= 2 * both
        far = jnp.where(above > below, 1, -1)
        sign = jnp.where(inner, jnp.where(k % 2 == 1, 1, -1), far)
        return self.z + sign * jnp.where(inner, (k + 1) // 2, k - both)


def remote(src, dst, send, recv, where):
    return pltpu.make_async_remote_copy(
        src_ref=src,
        dst_ref=dst,
        send_sem=send,
        recv_sem=recv,
        device_id=where,
        device_id_type=pl.DeviceIdType.MESH,
    )


class Gather:
    def __init__(self, net, buf, sems):
        self.net, self.buf = net, buf
        self.zs, self.zr, self.xs, self.xr, self.ys, self.yr, self.cs, self.cr = sems

    def block(self, k, kind, c=None):
        net = self.net
        x = net.ox if kind % 2 else net.x
        y = net.oy if kind // 2 else net.y
        return self.buf.at[net.near(k), x, y, net.c if c is None else c]

    def over_z(self, k):
        net, b = self.net, self.block(0, 0)
        return remote(b, b, self.zs.at[k - 1], self.zr.at[net.z], net.at(z=net.near(k)))

    def from_z(self, k):
        net, b = self.net, self.block(k, 0)
        return remote(b, b, self.zs.at[k - 1], self.zr.at[net.near(k)], net.at(z=net.near(k)))

    def over_x(self, k, arriving=False):
        b = self.block(k, 1 if arriving else 0)
        return remote(b, b, self.xs.at[k], self.xr.at[k], self.net.at(x=self.net.ox))

    def over_y(self, kind, k, arriving=False):
        b = self.block(k, kind + 2 if arriving else kind)
        return remote(b, b, self.ys.at[kind, k], self.yr.at[kind, k], self.net.at(y=self.net.oy))

    def over_c(self, kind, k, arriving=False):
        b = self.block(k, kind, self.net.oc if arriving else None)
        return remote(b, b, self.cs.at[kind, k], self.cr.at[kind, k], self.net.at(c=self.net.oc))

    def spread(self, k):
        self.over_y(0, k).start()
        self.over_x(k).start()
        self.over_c(0, k).start()

    def start(self):
        for k in range(1, self.net.zs):
            self.over_z(k).start()
        self.spread(0)

    def pass_z(self, k):
        self.from_z(k).wait_recv()
        self.spread(k)

    def pass_x(self, k):
        self.over_x(k, True).wait_recv()
        self.over_y(1, k).start()
        self.over_c(1, k).start()

    def pass_y(self, kind, k):
        self.over_y(kind, k, True).wait_recv()
        self.over_c(kind + 2, k).start()

    def finish(self):
        for k in range(self.net.zs):
            for kind in range(4):
                self.over_c(kind, k, True).wait_recv()

    def drain(self):
        for k in range(self.net.zs):
            if k:
                self.over_z(k).wait_send()
            self.over_x(k).wait_send()
            for kind in range(2):
                self.over_y(kind, k).wait_send()
            for kind in range(4):
                self.over_c(kind, k).wait_send()


class Exchange:
    def __init__(self, net, k_buf, v_buf, head_width, sems):
        self.net, self.bufs, self.head_width = net, (k_buf, v_buf), head_width
        self.zs, self.zr, self.xs, self.xr = sems

    def block(self, i, z, x):
        if i == 0:
            return self.bufs[0].at[z, x]
        return self.bufs[1].at[z, x, :, : self.head_width]

    def over_z(self, i, k):
        net = self.net
        b = self.block(i, net.z, net.x)
        return remote(b, b, self.zs.at[i, k - 1], self.zr.at[i, net.z], net.at(z=net.near(k)))

    def from_z(self, i, k):
        net = self.net
        z = net.near(k)
        b = self.block(i, z, net.x)
        return remote(b, b, self.zs.at[i, k - 1], self.zr.at[i, z], net.at(z=z))

    def over_x(self, i, k, arriving=False):
        net = self.net
        b = self.block(i, net.near(k), net.ox if arriving else net.x)
        return remote(b, b, self.xs.at[i, k], self.xr.at[i, k], net.at(x=net.ox))

    def send_z(self, k):
        for i in range(2):
            self.over_z(i, k).start()

    def send_x(self, k):
        for i in range(2):
            self.over_x(i, k).start()

    def pass_z(self, k):
        for i in range(2):
            self.from_z(i, k).wait_recv()
            self.over_x(i, k).start()

    def arrived(self, k):
        for i in range(2):
            self.over_x(i, k, True).wait_recv()

    def drain(self):
        for k in range(self.net.zs):
            for i in range(2):
                if k:
                    self.over_z(i, k).wait_send()
                self.over_x(i, k).wait_send()


def greet(net):
    barrier = pltpu.get_barrier_semaphore()
    others = [net.at(x=net.ox), net.at(y=net.oy), net.at(c=net.oc)]
    others += [net.at(z=net.near(k)) for k in range(1, net.zs)]
    for where in others:
        pl.semaphore_signal(barrier, inc=1, device_id=where, device_id_type=pl.DeviceIdType.MESH)
    pl.semaphore_wait(barrier, len(others))


def layer_kernel(
    dims, group, scale, head_width, tok_hbm, qw_ref, kw_ref, vw_ref, ow_ref, qg_ref, kg_ref,
    out_ref, tok_ref, wkv, wq, wo, q_ref, k_buf, v_buf, acc_ref, max_ref, att_ref,
    cos_ref, sin_ref, tok_sem, *sems
):
    net = Net(dims)
    rows, depth = tok_ref.shape
    pair = 2 * head_width
    kv_width = kw_ref.shape[1]
    groups = kv_width // head_width
    q_width = qw_ref.shape[1]
    width = 4 * head_width
    load = pltpu.make_async_copy(tok_hbm, tok_ref, tok_sem)
    load.start()
    me = (net.z, net.x, net.y, net.c)
    wkv[me + (slice(None), slice(0, kv_width))] = kw_ref[...]
    wkv[me + (slice(None), slice(kv_width, 2 * kv_width))] = vw_ref[...]
    wq[me] = qw_ref[...]
    wo[me] = ow_ref[...]
    kv_w, q_w, o_w = (
        Gather(net, buf, sems[8 * i : 8 * i + 8]) for i, buf in enumerate((wkv, wq, wo))
    )
    kv = Exchange(net, k_buf, v_buf, head_width, sems[24:])
    steps = net.zs
    greet(net)
    kv_w.start()
    q_w.start()

    lane = lax.broadcasted_iota(jnp.int32, (rows, pair), 1)
    at = lax.broadcasted_iota(jnp.int32, (rows, pair), 0) + (net.z * net.xs + net.x) * rows
    quarter = head_width // 4
    power = (lane % quarter).astype(jnp.float32) * (-math.log(rope_base) / quarter)
    spot = jnp.where(lane % head_width < 2 * quarter, at // GRID_W, at % GRID_W)
    angle = spot.astype(jnp.float32) * jnp.exp(power)
    first = lane % (2 * quarter) < quarter
    cos_ref[...] = jnp.cos(angle)
    sin_ref[...] = jnp.where(first, -jnp.sin(angle), jnp.sin(angle))

    q_ref[...] = jnp.zeros_like(q_ref)
    acc_ref[...] = jnp.zeros_like(acc_ref)
    max_ref[...] = jnp.full_like(max_ref, -jnp.inf)
    tail = v_buf.shape[3] - head_width
    v_buf[:, :, :, head_width:] = jnp.ones(v_buf.shape[:3] + (tail, rows), v_buf.dtype)
    load.wait()

    r = lax.broadcasted_iota(jnp.int32, (2 * width, width), 0) % width // head_width
    c = lax.broadcasted_iota(jnp.int32, (2 * width, width), 1) // head_width
    averager = jnp.where(r == c, 1.0 / head_width, 0.0).astype(jnp.bfloat16)
    wide_first = jnp.concatenate([first, first], axis=1)

    def twice(ref):
        return jnp.concatenate([ref[...]] * 2, axis=1)

    def product(buf, at):
        w = buf[:, :, :, :, :, at : at + width].reshape(depth, width)
        return jnp.dot(tok_ref[...], w, preferred_element_type=jnp.float32)

    def halves(t):
        high = t.astype(jnp.bfloat16)
        return high, (t - high.astype(jnp.float32)).astype(jnp.bfloat16)

    def turned(t, gain_ref):
        gain = jnp.concatenate([gain_ref[...]] * 4, axis=1)
        mean_sq = jnp.dot(
            jnp.concatenate(halves(t * t), axis=1), averager, preferred_element_type=jnp.float32
        )
        t = t * lax.rsqrt(mean_sq + epsilon) * gain
        other = jnp.where(
            wide_first, pltpu.roll(t, width - quarter, 1), pltpu.roll(t, quarter, 1)
        )
        return t * twice(cos_ref) + other * twice(sin_ref)

    for k in range(1, steps):
        kv_w.pass_z(k)
    for k in range(steps):
        kv_w.pass_x(k)
    for k in range(1, steps):
        q_w.pass_z(k)
    for k in range(steps):
        kv_w.pass_y(0, k)
    for k in range(steps):
        kv_w.pass_y(1, k)
    kv_w.finish()
    for j in range(kv_width // width):
        cols = slice(j * width, (j + 1) * width)
        k_buf[net.z, net.x, :, cols] = turned(product(wkv, j * width), kg_ref).astype(k_buf.dtype)
        v = product(wkv, kv_width + j * width).T.astype(v_buf.dtype)
        for i in range(width // head_width):
            v_buf[net.z, net.x, j * (width // head_width) + i, :head_width] = v[
                i * head_width : (i + 1) * head_width
            ]
    kv.send_z(1)
    kv.send_x(0)
    for k in range(2, steps):
        kv.send_z(k)
    for k in range(steps):
        q_w.pass_x(k)
    o_w.start()
    for k in range(steps):
        q_w.pass_y(0, k)
    kv.pass_z(1)
    for k in range(steps):
        q_w.pass_y(1, k)
    q_w.finish()

    for j in range(q_width // width):
        q = turned(product(wq, j * width), qg_ref).astype(jnp.bfloat16).astype(jnp.float32)
        q = (q * (scale * math.log2(math.e))).T
        g = j
        base = (g % 2) * head_width
        for i, part in enumerate(halves(q)):
            for n in range(group):
                q_ref[
                    g, i * pair + base : i * pair + base + head_width, n * rows : (n + 1) * rows
                ] = part[n * head_width : (n + 1) * head_width]

    chunk = width
    keys_now = net.xs * rows
    chunks = group * rows // chunk

    def attend(k, g):
        z = net.near(k)
        keys = k_buf[z, :, :, pl.ds(pl.multiple_of(g // 2 * pair, pair), pair)]
        keys = keys.reshape(keys_now, pair)
        keys = jnp.concatenate([keys, keys], axis=1)
        values = jnp.concatenate([v_buf[z, x, g] for x in range(net.xs)], axis=1)
        cols = [slice(n * chunk, (n + 1) * chunk) for n in range(chunks)]
        scores = [
            jnp.dot(keys, q_ref[g, :, at], preferred_element_type=jnp.float32) for at in cols
        ]
        for at, s in zip(cols, scores):
            old = max_ref[g, :, at]
            top = jnp.maximum(old, jnp.max(s, axis=0, keepdims=True))
            p = jnp.exp2(s - top).astype(values.dtype)
            max_ref[g, :, at] = top
            acc_ref[g, :, at] = acc_ref[g, :, at] * jnp.exp2(old - top) + jnp.dot(
                values, p, preferred_element_type=jnp.float32
            )

    events = {t: [] for t in range(steps * groups)}
    kv.arrived(0)
    for k in range(2, steps):
        events[(k - 2) * groups + 1].append((kv.pass_z, k))
    for k in range(1, steps):
        events[k * groups].append((kv.arrived, k))
        events[2 * groups - 2 + k].append((o_w.pass_z, k))
    for k in range(steps):
        events[2 * groups + 2 + k].append((o_w.pass_x, k))
        events[3 * groups].append((o_w.pass_y, 0, k))

    def step(t, carry):
        k, g = t // groups, t % groups
        for when, todo in events.items():
            if todo:

                @pl.when(t == when)
                def _():
                    for act, *where in todo:
                        act(*where)

        attend(k, g)
        return carry

    lax.fori_loop(0, steps * groups, step, 0)

    for g in range(groups):
        for n in range(0, group, 2):
            parts = []
            for i in (n, n + 1):
                cols = slice(i * rows, (i + 1) * rows)
                total = acc_ref[g, head_width : head_width + 1, cols]
                parts.append(acc_ref[g, :head_width, cols] / total)
            at = (g * group + n) * head_width
            att_ref[:, at : at + pair] = jnp.concatenate(parts, axis=0).T.astype(att_ref.dtype)
    for k in range(steps):
        o_w.pass_y(1, k)
    o_w.finish()
    blocks = depth // width

    def project(j, carry):
        zx = j * width // ow_ref.shape[0]
        per = net.ys * CORES
        w = wo[zx // (net.xs * per), zx // per % net.xs].reshape(per * ow_ref.shape[0], q_width)
        out_ref[:, pl.ds(pl.multiple_of(j * width, width), width)] = lax.dot_general(
            att_ref[...], w, (((1,), (1,)), ((), ())), preferred_element_type=jnp.float32
        ).astype(out_ref.dtype)
        return carry

    lax.fori_loop(0, blocks, project, 0)
    kv_w.drain()
    q_w.drain()
    o_w.drain()
    kv.drain()


def vmem():
    return pl.BlockSpec(memory_space=pltpu.VMEM)


def fast(dims, tokens, q_weight, k_weight, v_weight, out_weight, q_gain, k_gain):
    zs, xs, ys = dims
    rows_in = tokens[0]
    rows, depth = rows_in.shape
    head_width = q_gain.shape[0]
    q_width = out_weight.shape[0]
    kv_width = k_weight.shape[1]
    groups = kv_width // head_width
    group = q_width // kv_width
    pair = 2 * head_width
    own = q_weight.shape[0]
    sums = 16
    dma = pltpu.SemaphoreType.DMA
    bf16, f32 = jnp.bfloat16, jnp.float32
    gather_sems = [
        dma((zs,)), dma((zs,)), dma((zs,)), dma((zs,)),
        dma((2, zs)), dma((2, zs)), dma((4, zs)), dma((4, zs)),
    ]
    grid = (zs, xs, ys, CORES, own)
    out = pl.pallas_call(
        functools.partial(layer_kernel, dims, group, head_width ** (-0.5), head_width),
        out_shape=jax.ShapeDtypeStruct((rows, depth), bf16),
        in_specs=[pl.BlockSpec(memory_space=pl.ANY)] + [vmem()] * 6,
        out_specs=vmem(),
        scratch_shapes=[
            pltpu.VMEM((rows, depth), bf16),
            pltpu.VMEM(grid + (2 * kv_width,), bf16),
            pltpu.VMEM(grid + (q_width,), bf16),
            pltpu.VMEM(grid + (q_width,), bf16),
            pltpu.VMEM((groups, 2 * pair, group * rows), bf16),
            pltpu.VMEM((zs, xs, rows, kv_width), bf16),
            pltpu.VMEM((zs, xs, groups, head_width + sums, rows), bf16),
            pltpu.VMEM((groups, head_width + sums, group * rows), f32),
            pltpu.VMEM((groups, 1, group * rows), f32),
            pltpu.VMEM((rows, q_width), bf16),
            pltpu.VMEM((rows, pair), f32),
            pltpu.VMEM((rows, pair), f32),
            dma,
        ]
        + gather_sems * 3
        + [dma((2, zs)), dma((2, zs)), dma((2, zs)), dma((2, zs))],
        compiler_params=pltpu.CompilerParams(
            collective_id=0, has_side_effects=True, vmem_limit_bytes=VMEM_BYTES
        ),
        cost_estimate=pl.CostEstimate(
            flops=100_000_000_000, bytes_accessed=10_000_000, transcendentals=20_000_000
        ),
    )(
        rows_in, q_weight, k_weight, v_weight, out_weight.T,
        q_gain.reshape(1, head_width), k_gain.reshape(1, head_width),
    )
    return out[None]


def normalize(tensor, gain_vec):
    mean_sq = jnp.mean(tensor * tensor, axis=-1, keepdims=True)
    return tensor * lax.rsqrt(mean_sq + epsilon) * gain_vec


def rotate(tensor, offset):
    row_count = tensor.shape[0]
    head_width = tensor.shape[2]
    quarter = head_width // 4
    half_width = head_width // 2
    positions = jnp.arange(row_count, dtype=jnp.int32) + offset
    frequency = rope_base ** (-jnp.arange(quarter, dtype=jnp.float32) / quarter)

    def rotate_pair(segment, coords):
        angles = coords.astype(jnp.float32)[:, None] * frequency[None, :]
        cosine = jnp.cos(angles)[:, None, :]
        sine_val = jnp.sin(angles)[:, None, :]
        low_half = segment[..., :quarter]
        high_half = segment[..., quarter:]
        return jnp.concatenate(
            [low_half * cosine - high_half * sine_val, high_half * cosine + low_half * sine_val],
            axis=-1,
        )

    return jnp.concatenate(
        [
            rotate_pair(tensor[..., :half_width], positions // GRID_W),
            rotate_pair(tensor[..., half_width:], positions % GRID_W),
        ],
        axis=-1,
    )


def attend(query_rows, key_rows, value_rows):
    row_count, head_width = query_rows.shape
    block_rows = math.gcd(row_count, 512)
    score_scale = head_width ** (-0.5)

    def attend_block(segment):
        scores = (
            lax.dot_general(
                segment, key_rows, (((1,), (1,)), ((), ())), preferred_element_type=jnp.float32
            )
            * score_scale
        )
        row_max = jnp.max(scores, axis=-1, keepdims=True)
        weights = jnp.exp(scores - row_max)
        shares = (weights / jnp.sum(weights, axis=-1, keepdims=True)).astype(jnp.bfloat16)
        return jnp.dot(shares, value_rows, preferred_element_type=jnp.float32).astype(jnp.bfloat16)

    blocks = query_rows.reshape(row_count // block_rows, block_rows, head_width)
    return lax.map(attend_block, blocks).reshape(row_count, head_width)


def plain(tokens, q_weight, k_weight, v_weight, out_weight, q_gain, k_gain):
    rows_in = tokens[0]
    tok_count = rows_in.shape[0]
    head_width = q_gain.shape[0]
    q_width = out_weight.shape[0]
    kv_width = k_weight.shape[1]
    q_heads = q_width // head_width
    kv_heads = kv_width // head_width
    group_size = q_heads // kv_heads
    sp_count = lax.axis_size("sp")
    offset = lax.axis_index("sp") * tok_count
    weight_rows = (
        lax.all_gather(q_weight, ("sp", "dp"), axis=0, tiled=True),
        lax.all_gather(k_weight, ("sp", "dp"), axis=0, tiled=True),
        lax.all_gather(v_weight, ("sp", "dp"), axis=0, tiled=True),
    )
    query_raw, key_raw, value_raw = tuple(
        (
            jnp.dot(rows_in, rows_part, preferred_element_type=jnp.float32)
            for rows_part in weight_rows
        )
    )
    queries = rotate(
        normalize(query_raw.reshape(tok_count, q_heads, head_width), q_gain), offset
    ).astype(jnp.bfloat16)
    keys_rot = rotate(
        normalize(key_raw.reshape(tok_count, kv_heads, head_width), k_gain), offset
    ).astype(jnp.bfloat16)
    values_dev = value_raw.astype(jnp.bfloat16)
    keys_wide = jnp.broadcast_to(
        keys_rot[:, :, None, :], (tok_count, kv_heads, group_size, head_width)
    ).reshape(tok_count, q_width)
    values_wide = jnp.broadcast_to(
        values_dev.reshape(tok_count, kv_heads, 1, head_width),
        (tok_count, kv_heads, group_size, head_width),
    ).reshape(tok_count, q_width)
    q_local, k_local, v_local = (
        lax.all_to_all(
            queries.reshape(tok_count, q_width), "sp", split_axis=1, concat_axis=0, tiled=True
        ),
        lax.all_to_all(keys_wide, "sp", split_axis=1, concat_axis=0, tiled=True),
        lax.all_to_all(values_wide, "sp", split_axis=1, concat_axis=0, tiled=True),
    )
    local_heads = q_width // sp_count // head_width
    outputs = []
    for head_index in range(local_heads):
        low_col = head_index * head_width
        outputs.append(
            attend(
                q_local[:, low_col : low_col + head_width],
                k_local[:, low_col : low_col + head_width],
                v_local[:, low_col : low_col + head_width],
            )
        )
    head_results = jnp.concatenate(outputs, axis=1)
    attended = lax.all_to_all(head_results, "sp", split_axis=0, concat_axis=1, tiled=True)
    result = jnp.dot(
        attended,
        lax.all_gather(out_weight, ("sp", "dp"), axis=1, tiled=True),
        preferred_element_type=jnp.float32,
    ).astype(jnp.bfloat16)
    return result[None]


def solution(mesh):
    sp, dp = mesh.shape["sp"], mesh.shape["dp"]
    across = dp // CORES
    exchange = dp == 2 * CORES and sp % across == 0 and sp // across > 1
    body = functools.partial(fast, (sp // across, across, across)) if exchange else plain
    return jax.shard_map(
        body,
        mesh=mesh,
        in_specs=(
            P("dp", "sp", None),
            P(("sp", "dp"), None),
            P(("sp", "dp"), None),
            P(("sp", "dp"), None),
            P(None, ("sp", "dp")),
            P(),
            P(),
        ),
        out_specs=P("dp", "sp", None),
        check_vma=False,
    )
```

time: 135 us -> 110 us (0.81)
  between operations: 13.4 us -> 0.01 us
  matrix products: 5.4 us -> 0 us
  other arithmetic: 2.6 us -> 0 us
  Pallas kernels: 110 us -> 108 us
    dot_general x1 -> x0, matrix products: 5.4 us -> none  [fast(): result = jnp.dot(attended, out_full, preferred_element_type=jnp.float32)]
    unnamed x0 -> x1, local copies, waits for them, and re-layouts: none -> 2.73 us
    another operation x6 -> x0, local copies, waits for them, and re-layouts: 2.56 us -> none  [the longest x2 0.94 us: tables(): jnp.tile(cos, (1, width // head_width))]
    pallas_call x1, Pallas kernels: 110 us -> 108 us  [fast(): pl.pallas_call(functools.partial(layer_kernel, dims, group, head_width **...]
    concatenate x3 -> x0, other arithmetic: 1.64 us -> none  [the longest x1 1.62 us: fast(): own = jnp.concatenate([k_weight, v_weight, q_weight], axis=1)]
  transfers between devices with their start and end apart: 1 -> 0, of which waited for: 0 -> 0; matrix products, arithmetic and copies ran while one was open for 4% -> 0% of each run, Pallas kernels for 82% -> 0%
where the time goes in v1:
time: 110 us
  Pallas kernels  108 us (98%)
  local copies, waits for them, and re-layouts  2.73 us (2%)
    pallas_call x1, Pallas kernels, fast(): pl.pallas_call(functools.partial(layer_kernel, dims, group, head_width **...  108 us
    unnamed x1, local copies, waits for them, and re-layouts  2.73 us

profile of v1, /device:TPU:0, one launch (start us, length us, event | category | flops | bytes accessed | tf_op | source)
XLA Modules:
  0.0 110.3 jit_solution(14622563186629026894)
XLA Ops:
  0.0 107.6 %shard_map.73 = bf16[384,2048]{1,0:T(8,128)(2,1)} custom-call(bf16[384,2048]{1,0:T(8,128)(2,1)} %bitcast.6, bf16[64,1024]{1,0:T(8,128)(2,1)} %qw_ref.1, bf16[64,256]{1,0:T(8,128)(2,1)} %kw_ref.1, bf16[64,256]{1,0:T(8,128)(2,1)} %vw_ref.1, bf16[64,1024]{1,0:T(8,128)(2,1)} %bitcast.7, f32[1,64]{1,0:T(1,128)} %bitcast.8, f32[1,64]{1,0:T(1,128)} %bitcast.9), custom_call_target="tpu_custom_call" | custom-call | flops 99999997952 | bytes 10000000 | tf_op jit(solution)/shard_map/pallas_call | solution.py:401
  107.6 2.7 %copy.9 = bf16[1,384,2048]{2,1,0:T(8,128)(2,1)} copy(bf16[1,384,2048]{2,1,0:T(8,128)(2,1)} %bitcast.5) | data formatting | bytes 3145728

commit v2 on v1

--- a/solution.py
+++ b/solution.py
@@ -29,6 +29,9 @@
         y = self.y if y is None else y
         c = self.c if c is None else c
         return {"sp": z * self.xs + x, "dp": y * CORES + c}
+
+    def inside(self, z):
+        return jnp.logical_and(z >= 0, z < self.zs)
 
     def near(self, k):
         below, above = self.z, self.zs - 1 - self.z
@@ -51,8 +54,8 @@
 
 
 class Gather:
-    def __init__(self, net, buf, sems):
-        self.net, self.buf = net, buf
+    def __init__(self, net, buf, split, sems):
+        self.net, self.buf, self.split = net, buf, split
         self.zs, self.zr, self.xs, self.xr, self.ys, self.yr, self.cs, self.cr = sems
 
     def block(self, k, kind, c=None):
@@ -61,6 +64,12 @@
         y = net.oy if kind // 2 else net.y
         return self.buf.at[net.near(k), x, y, net.c if c is None else c]
 
+    def half(self, k, kind, h):
+        net, wide = self.net, self.buf.shape[-1] // 2
+        x = net.ox if kind % 2 else net.x
+        y = net.oy if kind // 2 else net.y
+        return self.buf.at[net.near(k), x, y, net.c, :, pl.ds(h * wide, wide)]
+
     def over_z(self, k):
         net, b = self.net, self.block(0, 0)
         return remote(b, b, self.zs.at[k - 1], self.zr.at[net.z], net.at(z=net.near(k)))
@@ -71,25 +80,33 @@
 
     def over_x(self, k, arriving=False):
         b = self.block(k, 1 if arriving else 0)
-        return remote(b, b, self.xs.at[k], self.xr.at[k], self.net.at(x=self.net.ox))
-
-    def over_y(self, kind, k, arriving=False):
-        b = self.block(k, kind + 2 if arriving else kind)
-        return remote(b, b, self.ys.at[kind, k], self.yr.at[kind, k], self.net.at(y=self.net.oy))
+        return remote(b, b, self.xs.at[0, k], self.xr.at[0, k], self.net.at(x=self.net.ox))
+
+    def half_x(self, k, arriving=False):
+        b = self.half(k, 3 if arriving else 2, 1)
+        return remote(b, b, self.xs.at[1, k], self.xr.at[1, k], self.net.at(x=self.net.ox))
+
+    def over_y(self, k, arriving=False):
+        b = self.block(k, 2 if arriving else 0)
+        return remote(b, b, self.ys.at[0, k], self.yr.at[0, k], self.net.at(y=self.net.oy))
+
+    def corner_y(self, k, arriving=False):
+        kind = 3 if arriving else 1
+        b = self.half(k, kind, 0) if self.split else self.block(k, kind)
+        return remote(b, b, self.ys.at[1, k], self.yr.at[1, k], self.net.at(y=self.net.oy))
 
     def over_c(self, kind, k, arriving=False):
         b = self.block(k, kind, self.net.oc if arriving else None)
         return remote(b, b, self.cs.at[kind, k], self.cr.at[kind, k], self.net.at(c=self.net.oc))
 
+    def start_z(self):
+        for k in reversed(range(1, self.net.zs)):
+            self.over_z(k).start()
+
     def spread(self, k):
-        self.over_y(0, k).start()
+        self.over_y(k).start()
         self.over_x(k).start()
         self.over_c(0, k).start()
-
-    def start(self):
-        for k in range(1, self.net.zs):
-            self.over_z(k).start()
-        self.spread(0)
 
     def pass_z(self, k):
         self.from_z(k).wait_recv()
@@ -97,12 +114,20 @@
 
     def pass_x(self, k):
         self.over_x(k, True).wait_recv()
-        self.over_y(1, k).start()
+        self.corner_y(k).start()
         self.over_c(1, k).start()
 
-    def pass_y(self, kind, k):
-        self.over_y(kind, k, True).wait_recv()
-        self.over_c(kind + 2, k).start()
+    def pass_y(self, k):
+        self.over_y(k, True).wait_recv()
+        if self.split:
+            self.half_x(k).start()
+        self.over_c(2, k).start()
+
+    def pass_corner(self, k):
+        self.corner_y(k, True).wait_recv()
+        if self.split:
+            self.half_x(k, True).wait_recv()
+        self.over_c(3, k).start()
 
     def finish(self):
         for k in range(self.net.zs):
@@ -114,66 +139,107 @@
             if k:
                 self.over_z(k).wait_send()
             self.over_x(k).wait_send()
-            for kind in range(2):
-                self.over_y(kind, k).wait_send()
+            self.over_y(k).wait_send()
+            self.corner_y(k).wait_send()
+            if self.split:
+                self.half_x(k).wait_send()
             for kind in range(4):
                 self.over_c(kind, k).wait_send()
 
 
-class Exchange:
-    def __init__(self, net, k_buf, v_buf, head_width, sems):
-        self.net, self.bufs, self.head_width = net, (k_buf, v_buf), head_width
-        self.zs, self.zr, self.xs, self.xr = sems
-
-    def block(self, i, z, x):
-        if i == 0:
-            return self.bufs[0].at[z, x]
-        return self.bufs[1].at[z, x, :, : self.head_width]
-
-    def over_z(self, i, k):
+class Chain:
+    def __init__(self, net, send, recv):
+        self.net, self.send, self.recv = net, send, recv
+
+    def own(self, side):
         net = self.net
-        b = self.block(i, net.z, net.x)
-        return remote(b, b, self.zs.at[i, k - 1], self.zr.at[i, net.z], net.at(z=net.near(k)))
-
-    def from_z(self, i, k):
+        to = net.z + (1 if side else -1)
+        b = self.part(net.z)
+        return to, remote(
+            b, b, self.send.at[net.zs * side], self.recv.at[net.z], net.at(z=to)
+        )
+
+    def arrival(self, k):
+        z = self.net.near(k)
+        b = self.part(z)
+        return remote(b, b, self.send.at[k], self.recv.at[z], self.net.at(z=z))
+
+    def onward(self, k):
         net = self.net
         z = net.near(k)
-        b = self.block(i, z, net.x)
-        return remote(b, b, self.zs.at[i, k - 1], self.zr.at[i, z], net.at(z=z))
-
-    def over_x(self, i, k, arriving=False):
+        to = net.z + jnp.where(z > net.z, -1, 1)
+        b = self.part(z)
+        return to, remote(b, b, self.send.at[k], self.recv.at[z], net.at(z=to))
+
+    def each(self, one, act):
+        to, copy = one
+
+        @pl.when(self.net.inside(to))
+        def _():
+            act(copy)
+
+    def start(self):
+        for side in range(2):
+            self.each(self.own(side), lambda copy: copy.start())
+
+    def receive(self, k):
+        self.arrival(k).wait_recv()
+        self.each(self.onward(k), lambda copy: copy.start())
+
+    def drain(self):
+        for side in range(2):
+            self.each(self.own(side), lambda copy: copy.wait_send())
+        for k in range(1, self.net.zs):
+            self.each(self.onward(k), lambda copy: copy.wait_send())
+
+
+class KeyChain(Chain):
+    def __init__(self, net, buf, own, rows, sems):
+        super().__init__(net, sems[0], sems[1])
+        self.buf, self.mine, self.rows = buf, own, rows
+        self.cs, self.cr, self.ss, self.sr = sems[2:]
+
+    def part(self, z, c=None):
+        c = self.net.c if c is None else c
+        if self.rows is None:
+            return self.buf.at[z, c]
+        return self.buf.at[z, c, :, : self.rows]
+
+    def swap(self, arriving=False):
         net = self.net
-        b = self.block(i, net.near(k), net.ox if arriving else net.x)
-        return remote(b, b, self.xs.at[i, k], self.xr.at[i, k], net.at(x=net.ox))
-
-    def send_z(self, k):
-        for i in range(2):
-            self.over_z(i, k).start()
-
-    def send_x(self, k):
-        for i in range(2):
-            self.over_x(i, k).start()
+        dst = self.part(net.z, None if arriving else net.x)
+        return remote(self.mine, dst, self.ss, self.sr, net.at(x=net.ox, c=net.oc))
+
+    def over_c(self, k, arriving=False):
+        net = self.net
+        b = self.part(net.near(k), net.oc if arriving else None)
+        return remote(b, b, self.cs.at[k], self.cr.at[k], net.at(c=net.oc))
+
+    def begin(self):
+        self.start()
+        self.over_c(0).start()
+
+    def pass_swap(self):
+        self.swap(True).wait_recv()
+        self.begin()
 
     def pass_z(self, k):
-        for i in range(2):
-            self.from_z(i, k).wait_recv()
-            self.over_x(i, k).start()
+        self.receive(k)
+        self.over_c(k).start()
 
     def arrived(self, k):
-        for i in range(2):
-            self.over_x(i, k, True).wait_recv()
+        self.over_c(k, True).wait_recv()
 
     def drain(self):
+        super().drain()
         for k in range(self.net.zs):
-            for i in range(2):
-                if k:
-                    self.over_z(i, k).wait_send()
-                self.over_x(i, k).wait_send()
+            self.over_c(k).wait_send()
 
 
 def greet(net):
     barrier = pltpu.get_barrier_semaphore()
     others = [net.at(x=net.ox), net.at(y=net.oy), net.at(c=net.oc)]
+    others += [net.at(x=net.ox, c=net.oc)]
     others += [net.at(z=net.near(k)) for k in range(1, net.zs)]
     for where in others:
         pl.semaphore_signal(barrier, inc=1, device_id=where, device_id_type=pl.DeviceIdType.MESH)
@@ -182,8 +248,8 @@
 
 def layer_kernel(
     dims, group, scale, head_width, tok_hbm, qw_ref, kw_ref, vw_ref, ow_ref, qg_ref, kg_ref,
-    out_ref, tok_ref, wkv, wq, wo, q_ref, k_buf, v_buf, acc_ref, max_ref, att_ref,
-    cos_ref, sin_ref, tok_sem, *sems
+    out_ref, tok_ref, wkv, wq0, wq1, wo, q_ref, k_buf, v_buf, acc_ref, max_ref, att_ref,
+    k_own, v_own, q_own, q_in, att_own, cos_ref, sin_ref, tok_sem, *sems
 ):
     net = Net(dims)
     rows, depth = tok_ref.shape
@@ -197,16 +263,22 @@
     me = (net.z, net.x, net.y, net.c)
     wkv[me + (slice(None), slice(0, kv_width))] = kw_ref[...]
     wkv[me + (slice(None), slice(kv_width, 2 * kv_width))] = vw_ref[...]
-    wq[me] = qw_ref[...]
+    half = q_width // 2
+    wq0[me] = qw_ref[:, :half]
+    wq1[me] = qw_ref[:, half:]
     wo[me] = ow_ref[...]
-    kv_w, q_w, o_w = (
-        Gather(net, buf, sems[8 * i : 8 * i + 8]) for i, buf in enumerate((wkv, wq, wo))
-    )
-    kv = Exchange(net, k_buf, v_buf, head_width, sems[24:])
+    kv_w = Gather(net, wkv, True, sems[0:8])
+    q_w = [Gather(net, buf, False, sems[8 * i : 8 * i + 8]) for i, buf in ((1, wq0), (2, wq1))]
+    o_w = Gather(net, wo, False, sems[24:32])
+    keys = KeyChain(net, k_buf, k_own, None, sems[32:38])
+    values = KeyChain(net, v_buf, v_own, head_width, sems[38:44])
+    q_send, q_recv, a_send, a_recv = sems[44:]
+    native = net.c == net.x
+    foreign = net.c != net.x
     steps = net.zs
     greet(net)
-    kv_w.start()
-    q_w.start()
+    kv_w.start_z()
+    kv_w.spread(0)
 
     lane = lax.broadcasted_iota(jnp.int32, (rows, pair), 1)
     at = lax.broadcasted_iota(jnp.int32, (rows, pair), 0) + (net.z * net.xs + net.x) * rows
@@ -254,41 +326,92 @@
 
     for k in range(1, steps):
         kv_w.pass_z(k)
+    q_w[0].start_z()
     for k in range(steps):
         kv_w.pass_x(k)
+        kv_w.pass_y(k)
+    q_w[0].spread(0)
+    q_w[1].start_z()
+    for k in range(steps):
+        kv_w.pass_corner(k)
     for k in range(1, steps):
-        q_w.pass_z(k)
+        q_w[0].pass_z(k)
+    q_w[0].pass_x(0)
+    kv_w.finish()
+    k_own[...] = turned(product(wkv, 0), kg_ref).astype(k_buf.dtype)
+    v_own[...] = product(wkv, kv_width).T.astype(v_buf.dtype).reshape(v_own.shape)
+
+    @pl.when(native)
+    def _():
+        k_buf[net.z, net.c] = k_own[...]
+        v_buf[net.z, net.c, :, :head_width] = v_own[...]
+        keys.begin()
+        values.begin()
+
+    @pl.when(foreign)
+    def _():
+        keys.swap().start()
+        values.swap().start()
+
+    for k in range(1, steps):
+        q_w[0].pass_x(k)
+    q_w[1].spread(0)
+    for k in range(1, steps):
+        q_w[1].pass_z(k)
     for k in range(steps):
-        kv_w.pass_y(0, k)
+        q_w[0].pass_y(k)
+
+    @pl.when(foreign)
+    def _():
+        keys.pass_swap()
+        values.pass_swap()
+
     for k in range(steps):
-        kv_w.pass_y(1, k)
-    kv_w.finish()
-    for j in range(kv_width // width):
-        cols = slice(j * width, (j + 1) * width)
-        k_buf[net.z, net.x, :, cols] = turned(product(wkv, j * width), kg_ref).astype(k_buf.dtype)
-        v = product(wkv, kv_width + j * width).T.astype(v_buf.dtype)
-        for i in range(width // head_width):
-            v_buf[net.z, net.x, j * (width // head_width) + i, :head_width] = v[
-                i * head_width : (i + 1) * head_width
-            ]
-    kv.send_z(1)
-    kv.send_x(0)
-    for k in range(2, steps):
-        kv.send_z(k)
+        q_w[0].pass_corner(k)
     for k in range(steps):
-        q_w.pass_x(k)
-    o_w.start()
-    for k in range(steps):
-        q_w.pass_y(0, k)
-    kv.pass_z(1)
-    for k in range(steps):
-        q_w.pass_y(1, k)
-    q_w.finish()
-
-    for j in range(q_width // width):
-        q = turned(product(wq, j * width), qg_ref).astype(jnp.bfloat16).astype(jnp.float32)
-        q = (q * (scale * math.log2(math.e))).T
-        g = j
+        q_w[1].pass_x(k)
+    q_w[0].finish()
+
+    def both(act, k):
+        getattr(keys, act)(k)
+        getattr(values, act)(k)
+
+    edge = jnp.logical_or(net.z == 0, net.z == net.zs - 1)
+
+    def early(act, inside, *where):
+        @pl.when(edge != inside)
+        def _():
+            act(*where)
+
+    def q_swap(g):
+        return remote(
+            q_own.at[g], q_in.at[g], q_send.at[g], q_recv.at[g], net.at(x=net.ox, c=net.oc)
+        )
+
+    def a_swap(g):
+        return remote(
+            att_own.at[g], att_ref.at[g], a_send.at[g], a_recv.at[g], net.at(x=net.ox, c=net.oc)
+        )
+
+    def project_queries(g):
+        w = (wq0, wq1)[g * width // half]
+        q = turned(product(w, g * width % half), qg_ref).astype(jnp.bfloat16)
+
+        @pl.when(native)
+        def _():
+            q_in[g] = q
+
+        @pl.when(foreign)
+        def _():
+            q_own[g] = q
+            q_swap(g).start()
+
+    def place_queries(g):
+        @pl.when(foreign)
+        def _():
+            q_swap(g).wait_recv()
+
+        q = (q_in[g].astype(jnp.float32) * (scale * math.log2(math.e))).T
         base = (g % 2) * head_width
         for i, part in enumerate(halves(q)):
             for n in range(group):
@@ -296,42 +419,89 @@
                     g, i * pair + base : i * pair + base + head_width, n * rows : (n + 1) * rows
                 ] = part[n * head_width : (n + 1) * head_width]
 
+    def later_queries():
+        for k in range(steps):
+            q_w[1].pass_y(k)
+        for k in range(steps):
+            q_w[1].pass_corner(k)
+        q_w[1].finish()
+        for g in range(groups // 2, groups):
+            project_queries(g)
+
+    def place_later():
+        for g in range(groups // 2, groups):
+            place_queries(g)
+
+    for g in range(groups // 2):
+        project_queries(g)
+
     chunk = width
     keys_now = net.xs * rows
     chunks = group * rows // chunk
 
     def attend(k, g):
         z = net.near(k)
-        keys = k_buf[z, :, :, pl.ds(pl.multiple_of(g // 2 * pair, pair), pair)]
-        keys = keys.reshape(keys_now, pair)
-        keys = jnp.concatenate([keys, keys], axis=1)
-        values = jnp.concatenate([v_buf[z, x, g] for x in range(net.xs)], axis=1)
+        k_now = k_buf[z, :, :, pl.ds(pl.multiple_of(g // 2 * pair, pair), pair)]
+        k_now = k_now.reshape(keys_now, pair)
+        k_now = jnp.concatenate([k_now, k_now], axis=1)
+        v_now = jnp.concatenate([v_buf[z, x, g] for x in range(net.xs)], axis=1)
         cols = [slice(n * chunk, (n + 1) * chunk) for n in range(chunks)]
         scores = [
-            jnp.dot(keys, q_ref[g, :, at], preferred_element_type=jnp.float32) for at in cols
+            jnp.dot(k_now, q_ref[g, :, at], preferred_element_type=jnp.float32) for at in cols
         ]
         for at, s in zip(cols, scores):
             old = max_ref[g, :, at]
             top = jnp.maximum(old, jnp.max(s, axis=0, keepdims=True))
-            p = jnp.exp2(s - top).astype(values.dtype)
+            p = jnp.exp2(s - top).astype(v_now.dtype)
             max_ref[g, :, at] = top
             acc_ref[g, :, at] = acc_ref[g, :, at] * jnp.exp2(old - top) + jnp.dot(
-                values, p, preferred_element_type=jnp.float32
+                v_now, p, preferred_element_type=jnp.float32
             )
 
     events = {t: [] for t in range(steps * groups)}
-    kv.arrived(0)
+    both("pass_z", 1)
+    early(both, True, "pass_z", 2)
+    o_w.start_z()
+    o_w.spread(0)
+    for g in range(groups // 2):
+        place_queries(g)
+    both("arrived", 0)
+    events[2].append((both, "arrived", 1))
+    events[2].append((later_queries,))
+    events[4].append((place_later,))
+    events[4].append((early, both, True, "pass_z", 3))
+    events[4].append((early, both, False, "pass_z", 2))
+    events[8].append((early, both, False, "pass_z", 3))
     for k in range(2, steps):
-        events[(k - 2) * groups + 1].append((kv.pass_z, k))
+        events[k * groups].append((both, "arrived", k))
     for k in range(1, steps):
-        events[k * groups].append((kv.arrived, k))
-        events[2 * groups - 2 + k].append((o_w.pass_z, k))
+        events[groups + 1].append((o_w.pass_z, k))
     for k in range(steps):
-        events[2 * groups + 2 + k].append((o_w.pass_x, k))
-        events[3 * groups].append((o_w.pass_y, 0, k))
+        events[2 * groups].append((o_w.pass_x, k))
+        events[2 * groups].append((o_w.pass_y, k))
+        events[3 * groups + k].append((o_w.pass_corner, k))
+
+    def settle(g):
+        parts = []
+        for n in range(group):
+            cols = slice(n * rows, (n + 1) * rows)
+            total = acc_ref[g, head_width : head_width + 1, cols]
+            parts.append(acc_ref[g, :head_width, cols] / total)
+        a = jnp.concatenate(parts, axis=0).T.astype(att_ref.dtype)
+
+        @pl.when(native)
+        def _():
+            att_ref[g] = a
+
+        @pl.when(foreign)
+        def _():
+            att_own[g] = a
+            a_swap(g).start()
 
     def step(t, carry):
-        k, g = t // groups, t % groups
+        head = t < 2 * groups
+        k = jnp.where(head, t % groups // 2, t // groups)
+        g = jnp.where(head, t // groups * 2 + t % 2, t % groups)
         for when, todo in events.items():
             if todo:
 
@@ -341,38 +511,43 @@
                         act(*where)
 
         attend(k, g)
+
+        @pl.when(k == steps - 1)
+        def _():
+            settle(g)
+
         return carry
 
     lax.fori_loop(0, steps * groups, step, 0)
 
-    for g in range(groups):
-        for n in range(0, group, 2):
-            parts = []
-            for i in (n, n + 1):
-                cols = slice(i * rows, (i + 1) * rows)
-                total = acc_ref[g, head_width : head_width + 1, cols]
-                parts.append(acc_ref[g, :head_width, cols] / total)
-            at = (g * group + n) * head_width
-            att_ref[:, at : at + pair] = jnp.concatenate(parts, axis=0).T.astype(att_ref.dtype)
-    for k in range(steps):
-        o_w.pass_y(1, k)
     o_w.finish()
-    blocks = depth // width
+    across = 2 * width
+
+    @pl.when(foreign)
+    def _():
+        for g in range(groups):
+            a_swap(g).wait_recv()
+
+    attended = jnp.concatenate([att_ref[g] for g in range(groups)], axis=1)
 
     def project(j, carry):
-        zx = j * width // ow_ref.shape[0]
-        per = net.ys * CORES
-        w = wo[zx // (net.xs * per), zx // per % net.xs].reshape(per * ow_ref.shape[0], q_width)
-        out_ref[:, pl.ds(pl.multiple_of(j * width, width), width)] = lax.dot_general(
-            att_ref[...], w, (((1,), (1,)), ((), ())), preferred_element_type=jnp.float32
+        w = wo[j].reshape(across, q_width)
+        out_ref[:, pl.ds(pl.multiple_of(j * across, across), across)] = lax.dot_general(
+            attended, w, (((1,), (1,)), ((), ())), preferred_element_type=jnp.float32
         ).astype(out_ref.dtype)
         return carry
 
-    lax.fori_loop(0, blocks, project, 0)
-    kv_w.drain()
-    q_w.drain()
-    o_w.drain()
-    kv.drain()
+    lax.fori_loop(0, depth // across, project, 0)
+    for part in (kv_w, *q_w, o_w, keys, values):
+        part.drain()
+
+    @pl.when(foreign)
+    def _():
+        keys.swap().wait_send()
+        values.swap().wait_send()
+        for g in range(groups):
+            q_swap(g).wait_send()
+            a_swap(g).wait_send()
 
 
 def vmem():
@@ -394,32 +569,40 @@
     dma = pltpu.SemaphoreType.DMA
     bf16, f32 = jnp.bfloat16, jnp.float32
     gather_sems = [
-        dma((zs,)), dma((zs,)), dma((zs,)), dma((zs,)),
+        dma((zs,)), dma((zs,)), dma((2, zs)), dma((2, zs)),
         dma((2, zs)), dma((2, zs)), dma((4, zs)), dma((4, zs)),
     ]
+    key_sems = [dma((zs + 1,)), dma((zs,)), dma((zs,)), dma((zs,)), dma, dma]
     grid = (zs, xs, ys, CORES, own)
     out = pl.pallas_call(
         functools.partial(layer_kernel, dims, group, head_width ** (-0.5), head_width),
-        out_shape=jax.ShapeDtypeStruct((rows, depth), bf16),
+        out_shape=pltpu.VMEM((rows, depth), bf16),
         in_specs=[pl.BlockSpec(memory_space=pl.ANY)] + [vmem()] * 6,
         out_specs=vmem(),
         scratch_shapes=[
             pltpu.VMEM((rows, depth), bf16),
             pltpu.VMEM(grid + (2 * kv_width,), bf16),
-            pltpu.VMEM(grid + (q_width,), bf16),
+            pltpu.VMEM(grid + (q_width // 2,), bf16),
+            pltpu.VMEM(grid + (q_width // 2,), bf16),
             pltpu.VMEM(grid + (q_width,), bf16),
             pltpu.VMEM((groups, 2 * pair, group * rows), bf16),
             pltpu.VMEM((zs, xs, rows, kv_width), bf16),
             pltpu.VMEM((zs, xs, groups, head_width + sums, rows), bf16),
             pltpu.VMEM((groups, head_width + sums, group * rows), f32),
             pltpu.VMEM((groups, 1, group * rows), f32),
-            pltpu.VMEM((rows, q_width), bf16),
+            pltpu.VMEM((groups, rows, group * head_width), bf16),
+            pltpu.VMEM((rows, kv_width), bf16),
+            pltpu.VMEM((groups, head_width, rows), bf16),
+            pltpu.VMEM((groups, rows, group * head_width), bf16),
+            pltpu.VMEM((groups, rows, group * head_width), bf16),
+            pltpu.VMEM((groups, rows, group * head_width), bf16),
             pltpu.VMEM((rows, pair), f32),
             pltpu.VMEM((rows, pair), f32),
             dma,
         ]
-        + gather_sems * 3
-        + [dma((2, zs)), dma((2, zs)), dma((2, zs)), dma((2, zs))],
+        + gather_sems * 4
+        + key_sems * 2
+        + [dma((groups,))] * 4,
         compiler_params=pltpu.CompilerParams(
             collective_id=0, has_side_effects=True, vmem_limit_bytes=VMEM_BYTES
         ),

time: 110 us -> 96 us (0.87)
  the two profiles are of different devices: /device:TPU:0 before, /device:TPU:9 now
where the time goes in v2:
time: 96 us; the launch traced here: 95.8 us
  Pallas kernels  94.7 us (99%)
  local copies, waits for them, and re-layouts  1.15 us (1%)
    pallas_call x1, Pallas kernels, fast(): pl.pallas_call(functools.partial(layer_kernel, dims, group, head_width **...  94.7 us

profile of v2, /device:TPU:9, one launch (start us, length us, event | category | flops | bytes accessed | tf_op | source)
XLA Modules:
  0.0 95.8 jit_solution(4210064027782249071)
XLA Ops:
  0.0 94.7 %shard_map.73 = bf16[384,2048]{1,0:T(8,128)(2,1)S(1)} custom-call(bf16[384,2048]{1,0:T(8,128)(2,1)} %bitcast.6, bf16[64,1024]{1,0:T(8,128)(2,1)} %qw_ref.1, bf16[64,256]{1,0:T(8,128)(2,1)} %kw_ref.1, bf16[64,256]{1,0:T(8,128)(2,1)} %vw_ref.1, bf16[64,1024]{1,0:T(8,128)(2,1)} %bitcast.7, f32[1,64]{1,0:T(1,128)} %bitcast.8, f32[1,64]{1,0:T(1,128)} %bitcast.9), custom_call_target="tpu_custom_call" | custom-call | flops 99999997952 | bytes 10000000 | tf_op jit(solution)/shard_map/pallas_call | solution.py:577
  94.7 1.1 %copy.9 = bf16[1,384,2048]{2,1,0:T(8,128)(2,1)} copy(bf16[1,384,2048]{2,1,0:T(8,128)(2,1)S(1)} %bitcast.5) | data formatting | bytes 3145728

commit v3 on v2

--- a/solution.py
+++ b/solution.py
@@ -72,32 +72,36 @@
 
     def over_z(self, k):
         net, b = self.net, self.block(0, 0)
-        return remote(b, b, self.zs.at[k - 1], self.zr.at[net.z], net.at(z=net.near(k)))
+        return remote(b, b, self.zs, self.zr.at[net.z], net.at(z=net.near(k)))
 
     def from_z(self, k):
         net, b = self.net, self.block(k, 0)
-        return remote(b, b, self.zs.at[k - 1], self.zr.at[net.near(k)], net.at(z=net.near(k)))
+        return remote(b, b, self.zs, self.zr.at[net.near(k)], net.at(z=net.near(k)))
 
     def over_x(self, k, arriving=False):
         b = self.block(k, 1 if arriving else 0)
-        return remote(b, b, self.xs.at[0, k], self.xr.at[0, k], self.net.at(x=self.net.ox))
+        return remote(b, b, self.xs, self.xr.at[0, k], self.net.at(x=self.net.ox))
 
     def half_x(self, k, arriving=False):
         b = self.half(k, 3 if arriving else 2, 1)
-        return remote(b, b, self.xs.at[1, k], self.xr.at[1, k], self.net.at(x=self.net.ox))
+        return remote(b, b, self.xs, self.xr.at[1, k], self.net.at(x=self.net.ox))
 
     def over_y(self, k, arriving=False):
         b = self.block(k, 2 if arriving else 0)
-        return remote(b, b, self.ys.at[0, k], self.yr.at[0, k], self.net.at(y=self.net.oy))
+        return remote(b, b, self.ys, self.yr.at[0, k], self.net.at(y=self.net.oy))
 
     def corner_y(self, k, arriving=False):
         kind = 3 if arriving else 1
         b = self.half(k, kind, 0) if self.split else self.block(k, kind)
-        return remote(b, b, self.ys.at[1, k], self.yr.at[1, k], self.net.at(y=self.net.oy))
-
-    def over_c(self, kind, k, arriving=False):
-        b = self.block(k, kind, self.net.oc if arriving else None)
-        return remote(b, b, self.cs.at[kind, k], self.cr.at[kind, k], self.net.at(c=self.net.oc))
+        return remote(b, b, self.ys, self.yr.at[1, k], self.net.at(y=self.net.oy))
+
+    def over_c(self, kind, k):
+        b = self.block(k, kind)
+        return remote(b, b, self.cs, self.cr, self.net.at(c=self.net.oc))
+
+    def bulk(self, sem, steps, xs=1, ys=1, wide=None):
+        b = self.buf.at[:steps, :xs, :ys, 0, :, :wide]
+        return remote(b, b, sem, self.cr, self.net.at(c=self.net.oc))
 
     def start_z(self):
         for k in reversed(range(1, self.net.zs)):
@@ -130,21 +134,19 @@
         self.over_c(3, k).start()
 
     def finish(self):
-        for k in range(self.net.zs):
-            for kind in range(4):
-                self.over_c(kind, k, True).wait_recv()
+        self.bulk(self.cs, self.net.zs, self.net.xs, self.net.ys).wait_recv()
 
     def drain(self):
-        for k in range(self.net.zs):
-            if k:
-                self.over_z(k).wait_send()
-            self.over_x(k).wait_send()
-            self.over_y(k).wait_send()
-            self.corner_y(k).wait_send()
-            if self.split:
-                self.half_x(k).wait_send()
-            for kind in range(4):
-                self.over_c(kind, k).wait_send()
+        net = self.net
+        self.bulk(self.zs, net.zs - 1).wait_send()
+        self.bulk(self.cs, net.zs, net.xs, net.ys).wait_send()
+        if self.split:
+            three = 3 * self.buf.shape[-1] // 4
+            self.bulk(self.xs, net.zs, net.xs, 1, three).wait_send()
+            self.bulk(self.ys, net.zs, 1, net.ys, three).wait_send()
+        else:
+            self.bulk(self.xs, net.zs).wait_send()
+            self.bulk(self.ys, net.zs, 1, net.ys).wait_send()
 
 
 class Chain:
@@ -249,7 +251,7 @@
 def layer_kernel(
     dims, group, scale, head_width, tok_hbm, qw_ref, kw_ref, vw_ref, ow_ref, qg_ref, kg_ref,
     out_ref, tok_ref, wkv, wq0, wq1, wo, q_ref, k_buf, v_buf, acc_ref, max_ref, att_ref,
-    k_own, v_own, q_own, q_in, att_own, cos_ref, sin_ref, tok_sem, *sems
+    k_own, v_own, q_own, q_in, att_own, sum_ref, cos_ref, sin_ref, tok_sem, *sems
 ):
     net = Net(dims)
     rows, depth = tok_ref.shape
@@ -279,6 +281,8 @@
     greet(net)
     kv_w.start_z()
     kv_w.spread(0)
+    q_w[0].spread(0)
+    q_w[1].spread(0)
 
     lane = lax.broadcasted_iota(jnp.int32, (rows, pair), 1)
     at = lax.broadcasted_iota(jnp.int32, (rows, pair), 0) + (net.z * net.xs + net.x) * rows
@@ -330,7 +334,6 @@
     for k in range(steps):
         kv_w.pass_x(k)
         kv_w.pass_y(k)
-    q_w[0].spread(0)
     q_w[1].start_z()
     for k in range(steps):
         kv_w.pass_corner(k)
@@ -355,7 +358,6 @@
 
     for k in range(1, steps):
         q_w[0].pass_x(k)
-    q_w[1].spread(0)
     for k in range(1, steps):
         q_w[1].pass_z(k)
     for k in range(steps):
@@ -366,10 +368,12 @@
         keys.pass_swap()
         values.pass_swap()
 
+    o_w.start_z()
     for k in range(steps):
         q_w[0].pass_corner(k)
     for k in range(steps):
         q_w[1].pass_x(k)
+    o_w.spread(0)
     q_w[0].finish()
 
     def both(act, k):
@@ -419,11 +423,13 @@
                     g, i * pair + base : i * pair + base + head_width, n * rows : (n + 1) * rows
                 ] = part[n * head_width : (n + 1) * head_width]
 
-    def later_queries():
+    def hand_on():
         for k in range(steps):
             q_w[1].pass_y(k)
         for k in range(steps):
             q_w[1].pass_corner(k)
+
+    def later_queries():
         q_w[1].finish()
         for g in range(groups // 2, groups):
             project_queries(g)
@@ -458,28 +464,45 @@
                 v_now, p, preferred_element_type=jnp.float32
             )
 
+    wave = [(k, g) for k in range(steps - 1) for g in range(groups // 2)]
+    late = range(groups // 2, groups)
+    wave += [(k, g) for g in late for k in range(steps - 2)]
+    wave += [(steps - 1, g) for g in range(groups // 2)]
+    wave += [(k, g) for g in late for k in range(steps - 2, steps)]
+    last = wave.index((steps - 1, 0))
+
+    def order(t):
+        at = [t == i for i in range(len(wave))]
+        pick = [sum(jnp.where(hit, w[i], 0) for hit, w in zip(at, wave)) for i in range(2)]
+        return pick
+
     events = {t: [] for t in range(steps * groups)}
     both("pass_z", 1)
     early(both, True, "pass_z", 2)
-    o_w.start_z()
-    o_w.spread(0)
     for g in range(groups // 2):
         place_queries(g)
     both("arrived", 0)
+    def only(who, act, *where):
+        @pl.when(who)
+        def _():
+            act(*where)
+
     events[2].append((both, "arrived", 1))
-    events[2].append((later_queries,))
-    events[4].append((place_later,))
+    events[3].append((hand_on,))
+    events[3].append((only, foreign, later_queries))
+    for k in range(1, steps):
+        events[3].append((o_w.pass_z, k))
     events[4].append((early, both, True, "pass_z", 3))
+    events[4].append((only, native, later_queries))
     events[4].append((early, both, False, "pass_z", 2))
-    events[8].append((early, both, False, "pass_z", 3))
-    for k in range(2, steps):
-        events[k * groups].append((both, "arrived", k))
-    for k in range(1, steps):
-        events[groups + 1].append((o_w.pass_z, k))
+    events[4].append((both, "arrived", 2))
+    events[6].append((place_later,))
+    events[9].append((early, both, False, "pass_z", 3))
+    events[last].append((both, "arrived", 3))
     for k in range(steps):
-        events[2 * groups].append((o_w.pass_x, k))
-        events[2 * groups].append((o_w.pass_y, k))
-        events[3 * groups + k].append((o_w.pass_corner, k))
+        events[7].append((o_w.pass_x, k))
+        events[9].append((o_w.pass_y, k))
+        events[12 + k].append((o_w.pass_corner, k))
 
     def settle(g):
         parts = []
@@ -499,9 +522,7 @@
             a_swap(g).start()
 
     def step(t, carry):
-        head = t < 2 * groups
-        k = jnp.where(head, t % groups // 2, t // groups)
-        g = jnp.where(head, t // groups * 2 + t % 2, t % groups)
+        k, g = order(t)
         for when, todo in events.items():
             if todo:
 
@@ -523,21 +544,35 @@
     o_w.finish()
     across = 2 * width
 
-    @pl.when(foreign)
-    def _():
-        for g in range(groups):
-            a_swap(g).wait_recv()
-
-    attended = jnp.concatenate([att_ref[g] for g in range(groups)], axis=1)
-
-    def project(j, carry):
-        w = wo[j].reshape(across, q_width)
-        out_ref[:, pl.ds(pl.multiple_of(j * across, across), across)] = lax.dot_general(
-            attended, w, (((1,), (1,)), ((), ())), preferred_element_type=jnp.float32
-        ).astype(out_ref.dtype)
-        return carry
-
-    lax.fori_loop(0, depth // across, project, 0)
+    def project(first, last):
+        attended = jnp.concatenate([att_ref[g] for g in range(first, last)], axis=1)
+        wide = group * head_width
+
+        def one(j, carry):
+            w = wo[j, :, :, :, :, first * wide : last * wide]
+            cols = pl.ds(pl.multiple_of(j * across, across), across)
+            part = lax.dot_general(
+                attended,
+                w.reshape(across, (last - first) * wide),
+                (((1,), (1,)), ((), ())),
+                preferred_element_type=jnp.float32,
+            )
+            if last < groups:
+                sum_ref[:, cols] = part
+            else:
+                out_ref[:, cols] = (sum_ref[:, cols] + part).astype(out_ref.dtype)
+            return carry
+
+        lax.fori_loop(0, depth // across, one, 0)
+
+    for first, last in ((0, groups - 1), (groups - 1, groups)):
+
+        @pl.when(foreign)
+        def _():
+            for g in range(first, last):
+                a_swap(g).wait_recv()
+
+        project(first, last)
     for part in (kv_w, *q_w, o_w, keys, values):
         part.drain()
 
@@ -569,8 +604,7 @@
     dma = pltpu.SemaphoreType.DMA
     bf16, f32 = jnp.bfloat16, jnp.float32
     gather_sems = [
-        dma((zs,)), dma((zs,)), dma((2, zs)), dma((2, zs)),
-        dma((2, zs)), dma((2, zs)), dma((4, zs)), dma((4, zs)),
+        dma, dma((zs,)), dma, dma((2, zs)), dma, dma((2, zs)), dma, dma,
     ]
     key_sems = [dma((zs + 1,)), dma((zs,)), dma((zs,)), dma((zs,)), dma, dma]
     grid = (zs, xs, ys, CORES, own)
@@ -596,6 +630,7 @@
             pltpu.VMEM((groups, rows, group * head_width), bf16),
             pltpu.VMEM((groups, rows, group * head_width), bf16),
             pltpu.VMEM((groups, rows, group * head_width), bf16),
+            pltpu.VMEM((rows, depth), f32),
             pltpu.VMEM((rows, pair), f32),
             pltpu.VMEM((rows, pair), f32),
             dma,

time: 96 us -> 87.1 us (0.907)
  the two profiles are of different devices: /device:TPU:9 before, /device:TPU:0 now
where the time goes in v3:
time: 87.1 us; the launch traced here: 86.3 us
  Pallas kernels  85.2 us (98%)
  local copies, waits for them, and re-layouts  1.15 us (1%)
    pallas_call x1, Pallas kernels, fast(): pl.pallas_call(functools.partial(layer_kernel, dims, group, head_width **...  85.2 us

profile of v3, /device:TPU:0, one launch (start us, length us, event | category | flops | bytes accessed | tf_op | source)
XLA Modules:
  0.0 86.3 jit_solution(7483353340492851799)
XLA Ops:
  0.0 85.2 %shard_map.73 = bf16[384,2048]{1,0:T(8,128)(2,1)S(1)} custom-call(bf16[384,2048]{1,0:T(8,128)(2,1)} %bitcast.6, bf16[64,1024]{1,0:T(8,128)(2,1)} %qw_ref.1, bf16[64,256]{1,0:T(8,128)(2,1)} %kw_ref.1, bf16[64,256]{1,0:T(8,128)(2,1)} %vw_ref.1, bf16[64,1024]{1,0:T(8,128)(2,1)} %bitcast.7, f32[1,64]{1,0:T(1,128)} %bitcast.8, f32[1,64]{1,0:T(1,128)} %bitcast.9), custom_call_target="tpu_custom_call" | custom-call | flops 99999997952 | bytes 10000000 | tf_op jit(solution)/shard_map/pallas_call | solution.py:611
  85.2 1.1 %copy.9 = bf16[1,384,2048]{2,1,0:T(8,128)(2,1)} copy(bf16[1,384,2048]{2,1,0:T(8,128)(2,1)S(1)} %bitcast.5) | data formatting | bytes 3145728
